TPU v7x, 32 devices: a whole 2x2x4 slice. The times are simulated.
32 devices in a mesh: sp: 4 (over y, x), tp: 8 (over z, core).
Axes of the slice: x: 2, y: 2, z: 4, core: 2. Of those that a mesh axis runs over, the one named last changes fastest.
Arguments:
- tokens: bfloat16 [2048, 4096], P('sp', 'tp'), may hold values from -6 to 6
- pre_gain: float32 [2, 4096], replicated, may hold values from 0.1 to 1.9
- w_value: bfloat16 [2, 4096, 4096], P(None, 'sp', 'tp'), may hold values from -0.09375 to 0.09375
- w_gate: bfloat16 [2, 4096, 4096], P(None, 'sp', 'tp'), may hold values from -0.09375 to 0.09375
- conv_taps: float32 [2, 31, 4096], P(None, None, 'tp'), may hold values from -3.5 to 3.5
- conv_bias: float32 [2, 4096], P(None, 'tp'), may hold values from -3 to 3
- norm_gain: float32 [2, 4096], P(None, 'tp'), may hold values from 0.1 to 1.9
- norm_bias: float32 [2, 4096], P(None, 'tp'), may hold values from -3 to 3
- w_out: bfloat16 [2, 4096, 4096], P(None, 'sp', 'tp'), may hold values from -0.09375 to 0.09375
- post_gain: float32 [2, 4096], P(None, 'tp'), may hold values from 0.1 to 1.9
Outputs:
- stream: bfloat16 [2048, 4096], P('sp', 'tp')
All inputs are finite; a program needn't handle non-finite values.
Results may differ from a plain program's by a relative error of at most 0.009.
Values may be sent and summed in bfloat16 or wider, within the bound.
A program may use at most 64 MiB of HBM per device.

v0:
```python
import jax
import jax.numpy as jnp
from jax import lax
from jax.sharding import PartitionSpec as P


def passed_along(value, axis, steps):
    count = lax.axis_size(axis)
    leading, last = (max(0, -steps), min(count, count - steps))
    return lax.ppermute(value, axis, [(source, source + steps) for source in range(leading, last)])


def shards(
    tokens, pre_gain, w_value, w_gate, conv_taps, conv_bias, norm_gain, norm_bias, w_out, post_gain
):
    layer_count = w_value.shape[0]
    tap_count = conv_taps.shape[1]
    channel_count = conv_taps.shape[2] * lax.axis_size("tp")
    model_width = tokens.shape[1] * lax.axis_size("tp")
    local_rows = tokens.shape[0]
    every_value, every_gate, every_out = (
        lax.all_gather(w_value, "sp", axis=1, tiled=True),
        lax.all_gather(w_gate, "sp", axis=1, tiled=True),
        lax.all_gather(w_out, "sp", axis=1, tiled=True),
    )
    stream = tokens
    for layer_index in range(layer_count):
        gathered = lax.all_gather(stream, "tp", axis=1, tiled=True)
        full_rows = gathered.astype(jnp.float32)
        scale_rows = lax.rsqrt(jnp.mean(full_rows * full_rows, axis=-1, keepdims=True) + 1e-06)
        normed = (full_rows * scale_rows * pre_gain[layer_index]).astype(jnp.bfloat16)
        value_block = every_value[layer_index]
        gate_block = every_gate[layer_index]
        out_block = every_out[layer_index]
        value_proj = jnp.dot(normed, value_block, preferred_element_type=jnp.float32)
        gate_proj = jnp.dot(normed, gate_block, preferred_element_type=jnp.float32)
        glu_out = (value_proj * jax.nn.sigmoid(gate_proj)).astype(jnp.bfloat16)
        earlier = passed_along(glu_out[local_rows - (tap_count - 1) :], "sp", 1)
        padded = jnp.concatenate([earlier, glu_out], axis=0).astype(jnp.float32)
        filtered = jnp.zeros(glu_out.shape, jnp.float32) + conv_bias[layer_index]
        for tap_index in range(tap_count):
            filtered = (
                filtered
                + padded[tap_index : tap_index + local_rows] * conv_taps[layer_index, tap_index]
            )
        channel_sum, channel_square = lax.psum(
            (jnp.sum(filtered, axis=-1), jnp.sum(filtered * filtered, axis=-1)), "tp"
        )
        centre = channel_sum / channel_count
        spread = jnp.maximum(channel_square / channel_count - centre * centre, 0.0)
        shaped = (filtered - centre[:, None]) * lax.rsqrt(spread + 1e-05)[:, None]
        mixed = jax.nn.silu(shaped * norm_gain[layer_index] + norm_bias[layer_index]).astype(
            jnp.bfloat16
        )
        whole_mixed = lax.all_gather(mixed, "tp", axis=1, tiled=True)
        branch_low = jnp.dot(whole_mixed, out_block, preferred_element_type=jnp.float32).astype(
            jnp.bfloat16
        )
        branch = lax.optimization_barrier(branch_low).astype(jnp.float32)
        total = lax.psum(jnp.sum(branch * branch, axis=-1), "tp")
        rescale = lax.rsqrt(total / model_width + 1e-06)[:, None]
        stream = (stream.astype(jnp.float32) + branch * rescale * post_gain[layer_index]).astype(
            jnp.bfloat16
        )
    return stream


def solution(mesh):
    in_specs = (
        P("sp", "tp"),
        P(),
        P(None, "sp", "tp"),
        P(None, "sp", "tp"),
        P(None, None, "tp"),
        P(None, "tp"),
        P(None, "tp"),
        P(None, "tp"),
        P(None, "sp", "tp"),
        P(None, "tp"),
    )
    out_specs = P("sp", "tp")
    return jax.shard_map(shards, mesh=mesh, in_specs=in_specs, out_specs=out_specs, check_vma=False)
```

profile of v0, /device:TPU:0, one launch (start us, length us, event | category | flops | bytes accessed | tf_op | source)
XLA Modules:
  0.0 551.2 jit_solution(2232420375245703278)
XLA Ops:
  9.6 49.0 %all-gather.8.cloned.1.call-done = bf16[512,4096]{1,0:T(8,128)(2,1)} async-done(((bf16[512,512]{1,0:T(8,128)(2,1)}), bf16[512,4096]{1,0:T(8,128)(2,1)}) %all-gather.8.cloned.1.call-update) | async-done | bytes 4194320 | tf_op jit(solution)/shard_map/all_gather | solution.py:28
  58.6 3.1 fusion
  61.7 85.1 %all-gather.12.cloned.1.call-done = bf16[2,4096,512]{2,1,0:T(8,128)(2,1)} async-done(((bf16[2,1024,512]{2,1,0:T(8,128)(2,1)}), bf16[2,4096,512]{2,1,0:T(8,128)(2,1)}) %all-gather.12.cloned.1.call-update) | async-done | bytes 8388624 | tf_op jit(solution)/shard_map/all_gather | solution.py:23
  146.7 6.0 %fusion.21 = f32[512,512]{1,0:T(8,128)S(1)} fusion(bf16[2,4096,512]{2,1,0:T(8,128)(2,1)} %all-gather.12.cloned.1.call-done, bf16[512,4096]{1,0:T(8,128)(2,1)} %all-gather.8.cloned.1.call-done, f32[4096]{0:T(1024)S(1)} %bitcast.122, f32[512]{0:T(512)S(1)} %add_rsqrt_fusion.5), kind=kOutput, calls=%fused_computation.35 | convolution fusion | flops 2156658688 | bytes 9455616 | tf_op jit(solution)/shard_map/dot_general | solution.py:36
  152.7 83.4 %all-gather.10.cloned.1.call-done = bf16[2,4096,512]{2,1,0:T(8,128)(2,1)} async-done(((bf16[2,1024,512]{2,1,0:T(8,128)(2,1)}), bf16[2,4096,512]{2,1,0:T(8,128)(2,1)}) %all-gather.10.cloned.1.call-update) | async-done | bytes 8388624 | tf_op jit(solution)/shard_map/all_gather | solution.py:22
  236.1 5.8 %fusion.23 = bf16[512,512]{1,0:T(8,128)(2,1)S(1)} fusion(f32[512,512]{1,0:T(8,128)S(1)} %fusion.21, bf16[2,4096,512]{2,1,0:T(8,128)(2,1)} %all-gather.10.cloned.1.call-done, bf16[512,4096]{1,0:T(8,128)(2,1)} %all-gather.8.cloned.1.call-done, f32[4096]{0:T(1024)S(1)} %bitcast.123, f32[512]{0:T(512)S(1)} %add_rsqrt_fusion.5), kind=kOutput, calls=%fused_computation.37 | convolution fusion | flops 2156396544 | bytes 9979904 | tf_op jit(solution)/shard_map/dot_general | solution.py:35
  242.0 3.4 collective-permute-start
  245.4 1.6 collective-permute-done
  247.1 5.0 fusion.101
  252.1 15.3 %all-reduce.1 = (f32[512]{0:T(512)S(1)}, f32[512]{0:T(512)S(1)}) all-reduce(f32[512]{0:T(512)S(1)} %get-tuple-element.8, f32[512]{0:T(512)S(1)} %get-tuple-element.7), channel_id=1, replica_groups=mesh['sp'=4,'tp'=8] {'tp'}, use_global_device_ids=true, to_apply=%region_4.0 | all-reduce | flops 1024 | bytes 8192 | tf_op jit(solution)/shard_map/psum | solution.py:46
  268.8 56.5 %all-gather.16.cloned.1.call-done = bf16[2,4096,512]{2,1,0:T(8,128)(2,1)} async-done(((bf16[2,1024,512]{2,1,0:T(8,128)(2,1)}), bf16[2,4096,512]{2,1,0:T(8,128)(2,1)}) %all-gather.16.cloned.1.call-update) | async-done | bytes 8388624 | tf_op jit(solution)/shard_map/all_gather | solution.py:24
  325.3 48.4 %all-gather.14.cloned.1.call-done = bf16[512,4096]{1,0:T(8,128)(2,1)} async-done(((bf16[512,512]{1,0:T(8,128)(2,1)}), bf16[512,4096]{1,0:T(8,128)(2,1)}) %all-gather.14.cloned.1.call-update) | async-done | bytes 4194320 | tf_op jit(solution)/shard_map/all_gather | solution.py:55
  373.7 5.8 %fusion.24 = bf16[512,512]{1,0:T(8,128)(2,1)S(1)} fusion(bf16[512,4096]{1,0:T(8,128)(2,1)} %all-gather.14.cloned.1.call-done, bf16[2,4096,512]{2,1,0:T(8,128)(2,1)} %all-gather.16.cloned.1.call-done), kind=kOutput, calls=%fused_computation.38 | convolution fusion | flops 2147745792 | bytes 8912896 | tf_op jit(solution)/shard_map/dot_general | solution.py:56
  379.6 14.8 %psum.44 = f32[512]{0:T(512)S(1)} all-reduce(f32[512]{0:T(512)S(1)} %fusion.30), channel_id=1, replica_groups=mesh['sp'=4,'tp'=8] {'tp'}, use_global_device_ids=true, to_apply=%region_6.7 | all-reduce | flops 512 | bytes 4096 | tf_op jit(solution)/shard_map/psum | solution.py:60
  395.8 44.7 %all-gather.18.cloned.1.call-done = bf16[512,4096]{1,0:T(8,128)(2,1)} async-done(((bf16[512,512]{1,0:T(8,128)(2,1)}), bf16[512,4096]{1,0:T(8,128)(2,1)}) %all-gather.18.cloned.1.call-update) | async-done | bytes 4194320 | tf_op jit(solution)/shard_map/all_gather | solution.py:28
  440.5 3.2 fusion.3
  443.9 5.0 fusion.19
  449.0 2.4 fusion.22
  451.4 3.4 collective-permute-start.1
  456.5 5.0 fusion.100
  461.6 13.7 %all-reduce = (f32[512]{0:T(512)S(1)}, f32[512]{0:T(512)S(1)}) all-reduce(f32[512]{0:T(512)S(1)} %get-tuple-element.6, f32[512]{0:T(512)S(1)} %get-tuple-element.5), channel_id=1, replica_groups=mesh['sp'=4,'tp'=8] {'tp'}, use_global_device_ids=true, to_apply=%region_11.12 | all-reduce | flops 1024 | bytes 8192 | tf_op jit(solution)/shard_map/psum | solution.py:46
  476.6 45.9 %all-gather.20.cloned.1.call-done = bf16[512,4096]{1,0:T(8,128)(2,1)} async-done(((bf16[512,512]{1,0:T(8,128)(2,1)}), bf16[512,4096]{1,0:T(8,128)(2,1)}) %all-gather.20.cloned.1.call-update) | async-done | bytes 4194320 | tf_op jit(solution)/shard_map/all_gather | solution.py:55
  522.5 5.8 %fusion.25 = bf16[512,512]{1,0:T(8,128)(2,1)S(1)} fusion(bf16[512,4096]{1,0:T(8,128)(2,1)} %all-gather.20.cloned.1.call-done, bf16[2,4096,512]{2,1,0:T(8,128)(2,1)} %all-gather.16.cloned.1.call-done), kind=kOutput, calls=%fused_computation.39 | convolution fusion | flops 2147745792 | bytes 8912896 | tf_op jit(solution)/shard_map/dot_general | solution.py:56
  528.5 14.8 %psum.47 = f32[512]{0:T(512)S(1)} all-reduce(f32[512]{0:T(512)S(1)} %fusion.34), channel_id=1, replica_groups=mesh['sp'=4,'tp'=8] {'tp'}, use_global_device_ids=true, to_apply=%region_13.14 | all-reduce | flops 512 | bytes 4096 | tf_op jit(solution)/shard_map/psum | solution.py:60
  (63 shorter events, 10.4 us)
Async XLA Ops:
  6.5 2.8 copy-start.5
  6.5 2.9 copy-start.6
  6.5 2.9 copy-start.3
  6.5 3.0 copy-start.4
  6.5 52.0 %all-gather.8.cloned.1.call-start = ((), (), s32[]{:S(2)}) async-start(), calls=%async_computation | async-start | bytes 4718592 | tf_op jit(solution)/shard_map/all_gather | solution.py:28
  7.3 139.5 %all-gather.12.cloned.1.call-start = ((), (), s32[]{:S(2)}) async-start(), calls=%async_computation.2 | async-start | bytes 10485760 | tf_op jit(solution)/shard_map/all_gather | solution.py:23
  8.0 228.1 %all-gather.10.cloned.1.call-start = ((), (), s32[]{:S(2)}) async-start(), calls=%async_computation.1 | async-start | bytes 10485760 | tf_op jit(solution)/shard_map/all_gather | solution.py:22
  8.8 316.6 %all-gather.16.cloned.1.call-start = ((), (), s32[]{:S(2)}) async-start(), calls=%async_computation.4 | async-start | bytes 10485760 | tf_op jit(solution)/shard_map/all_gather | solution.py:24
  9.3 364.3 %all-gather.14.cloned.1.call-start = ((), (), s32[]{:S(2)}) async-start(), calls=%async_computation.3 | async-start | bytes 4718592 | tf_op jit(solution)/shard_map/all_gather | solution.py:55
  152.7 92.6 %copy-start.7 = (f32[2,512]{1,0:T(2,128)S(1)}, f32[2,512]{1,0:T(2,128)}, u32[]{:S(2)}) copy-start(f32[2,512]{1,0:T(2,128)} %param.16) | copy-start | bytes 12292
  242.0 5.0 collective-permute-start
  247.1 21.7 %copy-start.8 = (f32[2,512]{1,0:T(2,128)S(1)}, f32[2,512]{1,0:T(2,128)}, u32[]{:S(2)}) copy-start(f32[2,512]{1,0:T(2,128)} %param.19) | copy-start | bytes 12292
  268.7 171.8 %all-gather.18.cloned.1.call-start = ((), (), s32[]{:S(2)}) async-start(), calls=%async_computation.5 | async-start | bytes 4718592 | tf_op jit(solution)/shard_map/all_gather | solution.py:28
  268.8 125.7 %copy-start.2 = (bf16[512,512]{1,0:T(8,128)(2,1)S(1)}, bf16[512,512]{1,0:T(8,128)(2,1)}, u32[]{:S(2)}) copy-start(bf16[512,512]{1,0:T(8,128)(2,1)} %param.10) | copy-start | bytes 1572868
  395.5 127.0 %all-gather.20.cloned.1.call-start = ((), (), s32[]{:S(2)}) async-start(), calls=%async_computation.6 | async-start | bytes 4718592 | tf_op jit(solution)/shard_map/all_gather | solution.py:55
  440.5 3.4 copy-start.1
  440.5 8.5 %slice-start = ((s8[8388608]{0:T(1024)(128)(4,1)}), s8[4194304]{0:T(1024)(128)(4,1)S(1)}, s32[]{:S(2)}) async-start(s8[8388608]{0:T(1024)(128)(4,1)} %bitcast.194), calls=%async_computation.7 | async-start | bytes 8388608
  443.9 5.0 slice-start.1
  451.4 5.0 collective-permute-start.1
  476.6 66.7 %copy-start = (bf16[512,512]{1,0:T(8,128)(2,1)S(1)}, bf16[512,512]{1,0:T(8,128)(2,1)}, u32[]{:S(2)}) copy-start(bf16[512,512]{1,0:T(8,128)(2,1)} %fusion.33) | copy-start | bytes 1572868
Sparse Core Ops, SparseCore 0:
  9.0 49.5 all-gather.7
  60.4 86.2 all-gather.11
  148.6 87.4 all-gather.9
  237.8 87.4 all-gather.15
  326.8 46.8 all-gather.13
  395.7 44.7 all-gather.17
  476.7 45.7 all-gather.19
where the time goes:
time: 551 us
  waiting for transfers between devices  419 us (76%)
  blocking collectives  58.7 us (11%)
  matrix products  30.8 us (6%)
  other arithmetic  21.7 us (4%)
  between operations  13.8 us (3%)
  starting transfers between devices  7.2 us (1%)
    all_gather x2, waiting for transfers between devices, shards(): whole_mixed = lax.all_gather(mixed, 'tp', axis=1, tiled=True)  94.2 us
    all_gather x2, waiting for transfers between devices, shards(): gathered = lax.all_gather(stream, 'tp', axis=1, tiled=True)  93.7 us
    all_gather x1, waiting for transfers between devices, shards(): lax.all_gather(w_gate, 'sp', axis=1, tiled=True)  85.1 us
    all_gather x1, waiting for transfers between devices, shards(): lax.all_gather(w_value, 'sp', axis=1, tiled=True)  83.4 us
    all_gather x1, waiting for transfers between devices, shards(): lax.all_gather(w_out, 'sp', axis=1, tiled=True)  56.5 us
    psum x2, blocking collectives, shards(): total = lax.psum(jnp.sum(branch * branch, axis=-1), 'tp')  29.6 us
    psum x2, blocking collectives, shards(): lax.psum((jnp.sum(filtered, axis=-1), jnp.sum(filtered * filtered, axis=-...  29.1 us
    dot_general x2, matrix products, shards(): jnp.dot(whole_mixed, out_block, preferred_element_type=jnp.float32)  11.6 us
  transfers between devices with their start and end apart: 9, of which 9 were waited for; matrix products, arithmetic and copies ran while one was open for 4% of the time, Pallas kernels for 0%

commit v1 on v0

--- a/solution.py
+++ b/solution.py
@@ -25,7 +25,16 @@
     )
     stream = tokens
     for layer_index in range(layer_count):
-        gathered = lax.all_gather(stream, "tp", axis=1, tiled=True)
+        axis_len = lax.axis_size("tp")
+        pages = [stream]
+        for j in tuple(range(axis_len - 1)):
+            current_value = lax.ppermute(
+                pages[-1], "tp", [(q, (q + 1) % axis_len) for q in range(axis_len)]
+            )
+            pages.append(current_value)
+        frame_out = jnp.concatenate(pages[::-1], axis=1)
+        left_arr = lax.axis_index("tp")
+        gathered = jnp.roll(frame_out, shift=(left_arr + 1) * stream.shape[1], axis=1)
         full_rows = gathered.astype(jnp.float32)
         scale_rows = lax.rsqrt(jnp.mean(full_rows * full_rows, axis=-1, keepdims=True) + 1e-06)
         normed = (full_rows * scale_rows * pre_gain[layer_index]).astype(jnp.bfloat16)

time: 551 us -> 529 us (0.960)
  waiting for transfers between devices: 419 us -> 394 us
    ppermute x0 -> x14, waiting for transfers between devices: none -> 146 us  [shards(): lax.ppermute(pages[-1], 'tp', [(q, (q + 1) % axis_len) for q in range(axi...]
    all_gather x2 -> x0, waiting for transfers between devices: 93.7 us -> none  [shards(): gathered = lax.all_gather(stream, 'tp', axis=1, tiled=True)]
    all_gather x1, waiting for transfers between devices: 85.1 us -> 8.54 us  [shards(): lax.all_gather(w_gate, 'sp', axis=1, tiled=True)]
  transfers between devices with their start and end apart: 9 -> 21, of which waited for: 9 -> 21; matrix products, arithmetic and copies ran while one was open for 4% -> 5% of each run, Pallas kernels for 0% -> 0%
where the time goes in v1:
time: 529 us
  waiting for transfers between devices  394 us (74%)
  blocking collectives  58.5 us (11%)
  matrix products  28.4 us (5%)
  other arithmetic  23.4 us (4%)
  between operations  13.6 us (3%)
  starting transfers between devices  7.53 us (1%)
    ppermute x14, waiting for transfers between devices, shards(): lax.ppermute(pages[-1], 'tp', [(q, (q + 1) % axis_len) for q in range(axi...  146 us
    all_gather x2, waiting for transfers between devices, shards(): whole_mixed = lax.all_gather(mixed, 'tp', axis=1, tiled=True)  94.4 us
    all_gather x1, waiting for transfers between devices, shards(): lax.all_gather(w_value, 'sp', axis=1, tiled=True)  83.3 us
    all_gather x1, waiting for transfers between devices, shards(): lax.all_gather(w_out, 'sp', axis=1, tiled=True)  56.4 us
    psum x2, blocking collectives, shards(): total = lax.psum(jnp.sum(branch * branch, axis=-1), 'tp')  29.6 us
    psum x2, blocking collectives, shards(): lax.psum((jnp.sum(filtered, axis=-1), jnp.sum(filtered * filtered, axis=-...  28.9 us
    dot_general x2, matrix products, shards(): jnp.dot(whole_mixed, out_block, preferred_element_type=jnp.float32)  11.6 us
  transfers between devices with their start and end apart: 21, of which 21 were waited for; matrix products, arithmetic and copies ran while one was open for 5% of the time, Pallas kernels for 0%

profile of v1, /device:TPU:0, one launch (start us, length us, event | category | flops | bytes accessed | tf_op | source)
XLA Modules:
  0.0 529.1 jit_solution(12006272173676621819)
XLA Ops:
  9.4 10.9 %collective-permute-done = bf16[512,512]{1,0:T(8,128)(2,1)S(1)} collective-permute-done((bf16[512,512]{1,0:T(8,128)(2,1)S(1)}, bf16[512,512]{1,0:T(8,128)(2,1)S(1)}, u32[]{:S(2)}, u32[]{:S(2)}) %collective-permute-start) | collective-permute-done | bytes 524320 | tf_op jit(solution)/shard_map/ppermute | solution.py:31
  20.3 10.4 %collective-permute-done.1 = bf16[512,512]{1,0:T(8,128)(2,1)S(1)} collective-permute-done((bf16[512,512]{1,0:T(8,128)(2,1)S(1)}, bf16[512,512]{1,0:T(8,128)(2,1)S(1)}, u32[]{:S(2)}, u32[]{:S(2)}) %collective-permute-start.1) | collective-permute-done | bytes 524320 | tf_op jit(solution)/shard_map/ppermute | solution.py:31
  30.7 10.4 %collective-permute-done.2 = bf16[512,512]{1,0:T(8,128)(2,1)S(1)} collective-permute-done((bf16[512,512]{1,0:T(8,128)(2,1)S(1)}, bf16[512,512]{1,0:T(8,128)(2,1)S(1)}, u32[]{:S(2)}, u32[]{:S(2)}) %collective-permute-start.2) | collective-permute-done | bytes 524320 | tf_op jit(solution)/shard_map/ppermute | solution.py:31
  41.1 10.4 %collective-permute-done.3 = bf16[512,512]{1,0:T(8,128)(2,1)S(1)} collective-permute-done((bf16[512,512]{1,0:T(8,128)(2,1)S(1)}, bf16[512,512]{1,0:T(8,128)(2,1)S(1)}, u32[]{:S(2)}, u32[]{:S(2)}) %collective-permute-start.3) | collective-permute-done | bytes 524320 | tf_op jit(solution)/shard_map/ppermute | solution.py:31
  51.5 10.4 %collective-permute-done.4 = bf16[512,512]{1,0:T(8,128)(2,1)S(1)} collective-permute-done((bf16[512,512]{1,0:T(8,128)(2,1)S(1)}, bf16[512,512]{1,0:T(8,128)(2,1)S(1)}, u32[]{:S(2)}, u32[]{:S(2)}) %collective-permute-start.4) | collective-permute-done | bytes 524320 | tf_op jit(solution)/shard_map/ppermute | solution.py:31
  62.0 10.4 %collective-permute-done.5 = bf16[512,512]{1,0:T(8,128)(2,1)} collective-permute-done((bf16[512,512]{1,0:T(8,128)(2,1)S(1)}, bf16[512,512]{1,0:T(8,128)(2,1)}, u32[]{:S(2)}, u32[]{:S(2)}) %collective-permute-start.5) | collective-permute-done | bytes 524320 | tf_op jit(solution)/shard_map/ppermute | solution.py:31
  72.5 10.6 %collective-permute-done.6 = bf16[512,512]{1,0:T(8,128)(2,1)} collective-permute-done((bf16[512,512]{1,0:T(8,128)(2,1)}, bf16[512,512]{1,0:T(8,128)(2,1)}, u32[]{:S(2)}, u32[]{:S(2)}) %collective-permute-start.6) | collective-permute-done | bytes 524320 | tf_op jit(solution)/shard_map/ppermute | solution.py:31
  90.9 8.5 %all-gather.8.cloned.1.call-done = bf16[2,4096,512]{2,1,0:T(8,128)(2,1)} async-done(((bf16[2,1024,512]{2,1,0:T(8,128)(2,1)}), bf16[2,4096,512]{2,1,0:T(8,128)(2,1)}) %all-gather.8.cloned.1.call-update) | async-done | bytes 8388624 | tf_op jit(solution)/shard_map/all_gather | solution.py:23
  99.4 6.0 %fusion.23 = f32[512,512]{1,0:T(8,128)S(1)} fusion(bf16[2,4096,512]{2,1,0:T(8,128)(2,1)} %all-gather.8.cloned.1.call-done, bf16[512,4096]{1,0:T(8,128)(2,1)} %get-tuple-element.19, f32[4096]{0:T(1024)S(1)} %bitcast.122, f32[512]{0:T(512)S(1)} %add_rsqrt_fusion.5), kind=kOutput, calls=%fused_computation.41 | convolution fusion | flops 2156658688 | bytes 9455616 | tf_op jit(solution)/shard_map/dot_general | solution.py:45
  105.5 83.3 %all-gather.6.cloned.1.call-done = bf16[2,4096,512]{2,1,0:T(8,128)(2,1)} async-done(((bf16[2,1024,512]{2,1,0:T(8,128)(2,1)}), bf16[2,4096,512]{2,1,0:T(8,128)(2,1)}) %all-gather.6.cloned.1.call-update) | async-done | bytes 8388624 | tf_op jit(solution)/shard_map/all_gather | solution.py:22
  204.8 15.3 %all-reduce.1 = (f32[512]{0:T(512)S(1)}, f32[512]{0:T(512)S(1)}) all-reduce(f32[512]{0:T(512)S(1)} %get-tuple-element.9, f32[512]{0:T(512)S(1)} %get-tuple-element.8), channel_id=1, replica_groups=mesh['sp'=4,'tp'=8] {'tp'}, use_global_device_ids=true, to_apply=%region_4.6 | all-reduce | flops 1024 | bytes 8192 | tf_op jit(solution)/shard_map/psum | solution.py:55
  221.7 56.4 %all-gather.12.cloned.1.call-done = bf16[2,4096,512]{2,1,0:T(8,128)(2,1)} async-done(((bf16[2,1024,512]{2,1,0:T(8,128)(2,1)}), bf16[2,4096,512]{2,1,0:T(8,128)(2,1)}) %all-gather.12.cloned.1.call-update) | async-done | bytes 8388624 | tf_op jit(solution)/shard_map/all_gather | solution.py:24
  278.2 48.4 %all-gather.10.cloned.1.call-done = bf16[512,4096]{1,0:T(8,128)(2,1)} async-done(((bf16[512,512]{1,0:T(8,128)(2,1)}), bf16[512,4096]{1,0:T(8,128)(2,1)}) %all-gather.10.cloned.1.call-update) | async-done | bytes 4194320 | tf_op jit(solution)/shard_map/all_gather | solution.py:64
  332.5 14.8 %psum.44 = f32[512]{0:T(512)S(1)} all-reduce(f32[512]{0:T(512)S(1)} %fusion.32), channel_id=1, replica_groups=mesh['sp'=4,'tp'=8] {'tp'}, use_global_device_ids=true, to_apply=%region_6.8 | all-reduce | flops 512 | bytes 4096 | tf_op jit(solution)/shard_map/psum | solution.py:69
  347.6 10.4 %collective-permute-done.8 = bf16[512,512]{1,0:T(8,128)(2,1)S(1)} collective-permute-done((bf16[512,512]{1,0:T(8,128)(2,1)S(1)}, bf16[512,512]{1,0:T(8,128)(2,1)S(1)}, u32[]{:S(2)}, u32[]{:S(2)}) %collective-permute-start.8) | collective-permute-done | bytes 524320 | tf_op jit(solution)/shard_map/ppermute | solution.py:31
  358.0 10.4 %collective-permute-done.9 = bf16[512,512]{1,0:T(8,128)(2,1)S(1)} collective-permute-done((bf16[512,512]{1,0:T(8,128)(2,1)S(1)}, bf16[512,512]{1,0:T(8,128)(2,1)S(1)}, u32[]{:S(2)}, u32[]{:S(2)}) %collective-permute-start.9) | collective-permute-done | bytes 524320 | tf_op jit(solution)/shard_map/ppermute | solution.py:31
  368.4 10.4 %collective-permute-done.10 = bf16[512,512]{1,0:T(8,128)(2,1)S(1)} collective-permute-done((bf16[512,512]{1,0:T(8,128)(2,1)S(1)}, bf16[512,512]{1,0:T(8,128)(2,1)S(1)}, u32[]{:S(2)}, u32[]{:S(2)}) %collective-permute-start.10) | collective-permute-done | bytes 524320 | tf_op jit(solution)/shard_map/ppermute | solution.py:31
  378.9 10.4 %collective-permute-done.11 = bf16[512,512]{1,0:T(8,128)(2,1)S(1)} collective-permute-done((bf16[512,512]{1,0:T(8,128)(2,1)S(1)}, bf16[512,512]{1,0:T(8,128)(2,1)S(1)}, u32[]{:S(2)}, u32[]{:S(2)}) %collective-permute-start.11) | collective-permute-done | bytes 524320 | tf_op jit(solution)/shard_map/ppermute | solution.py:31
  389.3 10.4 %collective-permute-done.12 = bf16[512,512]{1,0:T(8,128)(2,1)S(1)} collective-permute-done((bf16[512,512]{1,0:T(8,128)(2,1)S(1)}, bf16[512,512]{1,0:T(8,128)(2,1)S(1)}, u32[]{:S(2)}, u32[]{:S(2)}) %collective-permute-start.12) | collective-permute-done | bytes 524320 | tf_op jit(solution)/shard_map/ppermute | solution.py:31
  399.7 10.4 %collective-permute-done.13 = bf16[512,512]{1,0:T(8,128)(2,1)S(1)} collective-permute-done((bf16[512,512]{1,0:T(8,128)(2,1)S(1)}, bf16[512,512]{1,0:T(8,128)(2,1)S(1)}, u32[]{:S(2)}, u32[]{:S(2)}) %collective-permute-start.13) | collective-permute-done | bytes 524320 | tf_op jit(solution)/shard_map/ppermute | solution.py:31
  410.1 10.4 %collective-permute-done.14 = bf16[512,512]{1,0:T(8,128)(2,1)S(1)} collective-permute-done((bf16[512,512]{1,0:T(8,128)(2,1)S(1)}, bf16[512,512]{1,0:T(8,128)(2,1)S(1)}, u32[]{:S(2)}, u32[]{:S(2)}) %collective-permute-start.14) | collective-permute-done | bytes 524320 | tf_op jit(solution)/shard_map/ppermute | solution.py:31
  439.8 13.6 %all-reduce = (f32[512]{0:T(512)S(1)}, f32[512]{0:T(512)S(1)}) all-reduce(f32[512]{0:T(512)S(1)} %get-tuple-element.7, f32[512]{0:T(512)S(1)} %get-tuple-element.6), channel_id=1, replica_groups=mesh['sp'=4,'tp'=8] {'tp'}, use_global_device_ids=true, to_apply=%region_11.13 | all-reduce | flops 1024 | bytes 8192 | tf_op jit(solution)/shard_map/psum | solution.py:55
  454.7 46.0 %all-gather.14.cloned.1.call-done = bf16[512,4096]{1,0:T(8,128)(2,1)} async-done(((bf16[512,512]{1,0:T(8,128)(2,1)}), bf16[512,4096]{1,0:T(8,128)(2,1)}) %all-gather.14.cloned.1.call-update) | async-done | bytes 4194320 | tf_op jit(solution)/shard_map/all_gather | solution.py:64
  506.7 14.8 %psum.47 = f32[512]{0:T(512)S(1)} all-reduce(f32[512]{0:T(512)S(1)} %fusion.36), channel_id=1, replica_groups=mesh['sp'=4,'tp'=8] {'tp'}, use_global_device_ids=true, to_apply=%region_13.15 | all-reduce | flops 512 | bytes 4096 | tf_op jit(solution)/shard_map/psum | solution.py:69
  (102 shorter events, 61.9 us)
Async XLA Ops:
  6.5 55.4 %copy-start.1 = (f32[2,31,512]{2,0,1:T(2,128)S(1)}, f32[2,31,512]{2,0,1:T(2,128)}, u32[]{:S(2)}) copy-start(f32[2,31,512]{2,0,1:T(2,128)} %param.16) | copy-start | bytes 380932
  6.5 65.8 %copy-start.4 = (f32[2,512]{1,0:T(2,128)S(1)}, f32[2,512]{1,0:T(2,128)}, u32[]{:S(2)}) copy-start(f32[2,512]{1,0:T(2,128)} %param.19) | copy-start | bytes 12292
  6.5 92.9 %all-gather.8.cloned.1.call-start = ((), (), s32[]{:S(2)}) async-start(), calls=%async_computation.1 | async-start | bytes 10485760 | tf_op jit(solution)/shard_map/all_gather | solution.py:23
  7.3 181.5 %all-gather.6.cloned.1.call-start = ((), (), s32[]{:S(2)}) async-start(), calls=%async_computation | async-start | bytes 10485760 | tf_op jit(solution)/shard_map/all_gather | solution.py:22
  8.0 270.1 %all-gather.12.cloned.1.call-start = ((), (), s32[]{:S(2)}) async-start(), calls=%async_computation.3 | async-start | bytes 10485760 | tf_op jit(solution)/shard_map/all_gather | solution.py:24
  8.8 317.7 %all-gather.10.cloned.1.call-start = ((), (), s32[]{:S(2)}) async-start(), calls=%async_computation.2 | async-start | bytes 4718592 | tf_op jit(solution)/shard_map/all_gather | solution.py:64
  8.8 11.4 %collective-permute-start = (bf16[512,512]{1,0:T(8,128)(2,1)S(1)}, bf16[512,512]{1,0:T(8,128)(2,1)S(1)}, u32[]{:S(2)}, u32[]{:S(2)}) collective-permute-start(bf16[512,512]{1,0:T(8,128)(2,1)S(1)} %copy-done), channel_id=1, source_target_pairs={{0,1},{1,2},{2,3},{3,4},{4,5},{5,6},{6,7},{7,0},{8,9},{9,10},{10,1... | collective-permute-start | bytes 1572872 | tf_op jit(solution)/shard_map/ppermute | solution.py:31
  20.3 10.4 %collective-permute-start.1 = (bf16[512,512]{1,0:T(8,128)(2,1)S(1)}, bf16[512,512]{1,0:T(8,128)(2,1)S(1)}, u32[]{:S(2)}, u32[]{:S(2)}) collective-permute-start(bf16[512,512]{1,0:T(8,128)(2,1)S(1)} %collective-permute-done), channel_id=1, source_target_pairs={{0,1},{1,2},{2,3},{3,4},{4,5},{5,6},{6,7},{7,0},{8,9},{9,10},{10,1... | collective-permute-start | bytes 1572872 | tf_op jit(solution)/shard_map/ppermute | solution.py:31
  30.7 10.4 %collective-permute-start.2 = (bf16[512,512]{1,0:T(8,128)(2,1)S(1)}, bf16[512,512]{1,0:T(8,128)(2,1)S(1)}, u32[]{:S(2)}, u32[]{:S(2)}) collective-permute-start(bf16[512,512]{1,0:T(8,128)(2,1)S(1)} %collective-permute-done.1), channel_id=1, source_target_pairs={{0,1},{1,2},{2,3},{3,4},{4,5},{5,6},{6,7},{7,0},{8,9},{9,10},{10,1... | collective-permute-start | bytes 1572872 | tf_op jit(solution)/shard_map/ppermute | solution.py:31
  41.1 10.4 %collective-permute-start.3 = (bf16[512,512]{1,0:T(8,128)(2,1)S(1)}, bf16[512,512]{1,0:T(8,128)(2,1)S(1)}, u32[]{:S(2)}, u32[]{:S(2)}) collective-permute-start(bf16[512,512]{1,0:T(8,128)(2,1)S(1)} %collective-permute-done.2), channel_id=1, source_target_pairs={{0,1},{1,2},{2,3},{3,4},{4,5},{5,6},{6,7},{7,0},{8,9},{9,10},{10,1... | collective-permute-start | bytes 1572872 | tf_op jit(solution)/shard_map/ppermute | solution.py:31
  51.5 10.4 %collective-permute-start.4 = (bf16[512,512]{1,0:T(8,128)(2,1)S(1)}, bf16[512,512]{1,0:T(8,128)(2,1)S(1)}, u32[]{:S(2)}, u32[]{:S(2)}) collective-permute-start(bf16[512,512]{1,0:T(8,128)(2,1)S(1)} %collective-permute-done.3), channel_id=1, source_target_pairs={{0,1},{1,2},{2,3},{3,4},{4,5},{5,6},{6,7},{7,0},{8,9},{9,10},{10,1... | collective-permute-start | bytes 1572872 | tf_op jit(solution)/shard_map/ppermute | solution.py:31
  61.9 10.5 %collective-permute-start.5 = (bf16[512,512]{1,0:T(8,128)(2,1)S(1)}, bf16[512,512]{1,0:T(8,128)(2,1)}, u32[]{:S(2)}, u32[]{:S(2)}) collective-permute-start(bf16[512,512]{1,0:T(8,128)(2,1)S(1)} %collective-permute-done.4), channel_id=1, source_target_pairs={{0,1},{1,2},{2,3},{3,4},{4,5},{5,6},{6,7},{7,0},{8,9},{9,10},{10,1... | collective-permute-start | bytes 1572872 | tf_op jit(solution)/shard_map/ppermute | solution.py:31
  72.4 10.7 %collective-permute-start.6 = (bf16[512,512]{1,0:T(8,128)(2,1)}, bf16[512,512]{1,0:T(8,128)(2,1)}, u32[]{:S(2)}, u32[]{:S(2)}) collective-permute-start(bf16[512,512]{1,0:T(8,128)(2,1)} %collective-permute-done.5), channel_id=1, source_target_pairs={{0,1},{1,2},{2,3},{3,4},{4,5},{5,6},{6,7},{7,0},{8,9},{9,10},{10,1... | collective-permute-start | bytes 1572872 | tf_op jit(solution)/shard_map/ppermute | solution.py:31
  105.4 92.6 %copy-start.5 = (f32[2,512]{1,0:T(2,128)S(1)}, f32[2,512]{1,0:T(2,128)}, u32[]{:S(2)}) copy-start(f32[2,512]{1,0:T(2,128)} %param.18) | copy-start | bytes 12292
  194.7 5.0 collective-permute-start.7
  221.5 279.3 %all-gather.14.cloned.1.call-start = ((), (), s32[]{:S(2)}) async-start(), calls=%async_computation.4 | async-start | bytes 4718592 | tf_op jit(solution)/shard_map/all_gather | solution.py:64
  347.6 10.5 %collective-permute-start.8 = (bf16[512,512]{1,0:T(8,128)(2,1)S(1)}, bf16[512,512]{1,0:T(8,128)(2,1)S(1)}, u32[]{:S(2)}, u32[]{:S(2)}) collective-permute-start(bf16[512,512]{1,0:T(8,128)(2,1)S(1)} %fusion.35), channel_id=1, source_target_pairs={{0,1},{1,2},{2,3},{3,4},{4,5},{5,6},{6,7},{7,0},{8,9},{9,10},{10,1... | collective-permute-start | bytes 1572872 | tf_op jit(solution)/shard_map/ppermute | solution.py:31
  358.0 10.4 %collective-permute-start.9 = (bf16[512,512]{1,0:T(8,128)(2,1)S(1)}, bf16[512,512]{1,0:T(8,128)(2,1)S(1)}, u32[]{:S(2)}, u32[]{:S(2)}) collective-permute-start(bf16[512,512]{1,0:T(8,128)(2,1)S(1)} %collective-permute-done.8), channel_id=1, source_target_pairs={{0,1},{1,2},{2,3},{3,4},{4,5},{5,6},{6,7},{7,0},{8,9},{9,10},{10,1... | collective-permute-start | bytes 1572872 | tf_op jit(solution)/shard_map/ppermute | solution.py:31
  368.4 10.4 %collective-permute-start.10 = (bf16[512,512]{1,0:T(8,128)(2,1)S(1)}, bf16[512,512]{1,0:T(8,128)(2,1)S(1)}, u32[]{:S(2)}, u32[]{:S(2)}) collective-permute-start(bf16[512,512]{1,0:T(8,128)(2,1)S(1)} %collective-permute-done.9), channel_id=1, source_target_pairs={{0,1},{1,2},{2,3},{3,4},{4,5},{5,6},{6,7},{7,0},{8,9},{9,10},{10,1... | collective-permute-start | bytes 1572872 | tf_op jit(solution)/shard_map/ppermute | solution.py:31
  378.8 10.4 %collective-permute-start.11 = (bf16[512,512]{1,0:T(8,128)(2,1)S(1)}, bf16[512,512]{1,0:T(8,128)(2,1)S(1)}, u32[]{:S(2)}, u32[]{:S(2)}) collective-permute-start(bf16[512,512]{1,0:T(8,128)(2,1)S(1)} %collective-permute-done.10), channel_id=1, source_target_pairs={{0,1},{1,2},{2,3},{3,4},{4,5},{5,6},{6,7},{7,0},{8,9},{9,10},{10,1... | collective-permute-start | bytes 1572872 | tf_op jit(solution)/shard_map/ppermute | solution.py:31
  389.3 10.4 %collective-permute-start.12 = (bf16[512,512]{1,0:T(8,128)(2,1)S(1)}, bf16[512,512]{1,0:T(8,128)(2,1)S(1)}, u32[]{:S(2)}, u32[]{:S(2)}) collective-permute-start(bf16[512,512]{1,0:T(8,128)(2,1)S(1)} %collective-permute-done.11), channel_id=1, source_target_pairs={{0,1},{1,2},{2,3},{3,4},{4,5},{5,6},{6,7},{7,0},{8,9},{9,10},{10,1... | collective-permute-start | bytes 1572872 | tf_op jit(solution)/shard_map/ppermute | solution.py:31
  399.7 10.4 %collective-permute-start.13 = (bf16[512,512]{1,0:T(8,128)(2,1)S(1)}, bf16[512,512]{1,0:T(8,128)(2,1)S(1)}, u32[]{:S(2)}, u32[]{:S(2)}) collective-permute-start(bf16[512,512]{1,0:T(8,128)(2,1)S(1)} %collective-permute-done.12), channel_id=1, source_target_pairs={{0,1},{1,2},{2,3},{3,4},{4,5},{5,6},{6,7},{7,0},{8,9},{9,10},{10,1... | collective-permute-start | bytes 1572872 | tf_op jit(solution)/shard_map/ppermute | solution.py:31
  410.1 10.4 %collective-permute-start.14 = (bf16[512,512]{1,0:T(8,128)(2,1)S(1)}, bf16[512,512]{1,0:T(8,128)(2,1)S(1)}, u32[]{:S(2)}, u32[]{:S(2)}) collective-permute-start(bf16[512,512]{1,0:T(8,128)(2,1)S(1)} %collective-permute-done.13), channel_id=1, source_target_pairs={{0,1},{1,2},{2,3},{3,4},{4,5},{5,6},{6,7},{7,0},{8,9},{9,10},{10,1... | collective-permute-start | bytes 1572872 | tf_op jit(solution)/shard_map/ppermute | solution.py:31
  429.9 4.7 collective-permute-start.15
  (8 other events, 152.1 us)
Sparse Core Ops, SparseCore 0:
  9.2 90.1 all-gather.7
  101.3 87.4 all-gather.5
  190.6 87.4 all-gather.11
  279.6 46.8 all-gather.9
  454.8 45.8 all-gather.13
